TPU v7x, 32 devices: a whole 2x2x4 slice. The times are simulated.
32 devices in a mesh: dp: 4 (over y, x), kv: 4 (over z), tp: 2 (over core).
Axes of the slice: x: 2, y: 2, z: 4, core: 2. Of those that a mesh axis runs over, the one named last changes fastest.
Arguments:
- piece_tokens: bfloat16 [256, 2048], P(('dp', 'kv')), parts along dimension 0, may hold values from -6 to 6
- dec_tokens: bfloat16 [192, 4, 2048], P(('dp', 'kv')), parts along dimension 0, may hold values from -6 to 6
- norm_gain: float32 [2048], replicated, may hold values from 0.1 to 1.9
- query_weight: bfloat16 [2048, 1024], P(None, 'tp'), may hold values from -0.375 to 0.375
- key_weight: bfloat16 [2048, 256], P(None, 'tp'), may hold values from -0.125 to 0.125
- value_weight: bfloat16 [2048, 256], P(None, 'tp'), may hold values from -0.125 to 0.125
- gate_weight: bfloat16 [2048, 8], P(None, 'tp'), may hold values from -0.125 to 0.125
- gate_bias: float32 [8], P('tp'), may hold values from 3.4 to 11
- out_weight: bfloat16 [1024, 2048], P('tp'), may hold values from -0.1875 to 0.1875
- out_gain: float32 [2048], replicated, may hold values from 0.1 to 1.9
- past_keys: bfloat16 [4096, 2, 128], P(('dp', 'kv'), 'tp'), parts along dimension 0, may hold values from -41 to 41
- past_values: bfloat16 [4096, 2, 128], P(('dp', 'kv'), 'tp'), parts along dimension 0, may hold values from -6 to 6
- past_gate: float32 [8, 4096], P('tp', ('dp', 'kv')), parts along dimension 1, may hold values from -1024 to 0
- dec_keys: bfloat16 [192, 512, 2, 128], P(('dp', 'kv'), None, 'tp'), parts along dimension 0, may hold values from -41 to 41
- dec_values: bfloat16 [192, 512, 2, 128], P(('dp', 'kv'), None, 'tp'), parts along dimension 0, may hold values from -6 to 6
- dec_gate: float32 [192, 8, 512], P(('dp', 'kv'), 'tp'), parts along dimension 0, may hold values from -512 to 0
- dec_lengths: int32 [192], P(('dp', 'kv')), parts along dimension 0, may hold values from 1 to 512, as said below
Outputs:
- piece_out: bfloat16 [256, 2048], P(('dp', 'kv')), parts along dimension 0
- dec_out: bfloat16 [192, 4, 2048], P(('dp', 'kv')), parts along dimension 0
There are 4 independent parts, one for each index of `dp`. A program takes and returns all parts, laid end to end along the dimension named above; an argument that names none is the same for every part. Nothing has to cross between parts.
Inputs may be any that keep to these rules, and one draw needn't show every extreme that they name: `dec_lengths`: some decoding sequence has all 512 slots live in every draw.
All inputs are finite; a program needn't handle non-finite values.
Results may differ from a plain program's by a relative error of at most 0.015.
Values may be sent and summed in bfloat16 or wider, within the bound.
A program may use at most 64 MiB of HBM per device.

v0:
```python
import jax
import jax.numpy as jnp
from jax import lax
from jax.sharding import PartitionSpec as P

EPS = 1e-06


def rms_scale(source, scale_gain):
    widened = source.astype(jnp.float32)
    return (
        widened * lax.rsqrt(jnp.mean(widened * widened, axis=-1, keepdims=True) + EPS) * scale_gain
    )


def body(
    piece_tokens,
    dec_tokens,
    norm_gain,
    query_weight,
    key_weight,
    value_weight,
    gate_weight,
    gate_bias,
    out_weight,
    out_gain,
    past_keys,
    past_values,
    past_gate,
    dec_keys,
    dec_values,
    dec_gate,
    dec_lengths,
):
    piece_rows = piece_tokens.shape[0]
    model_width = piece_tokens.shape[1]
    kv_local = past_keys.shape[1]
    head_dim = past_keys.shape[2]
    heads_local = gate_bias.shape[0]
    group_size = heads_local // kv_local
    score_scale = head_dim ** (-0.5)
    seq_count = dec_tokens.shape[0]
    new_count = dec_tokens.shape[1]
    kv_count = lax.axis_size("kv")
    position = lax.axis_index("kv")
    all_rows = jnp.concatenate(
        [piece_tokens, dec_tokens.reshape(seq_count * new_count, model_width)], axis=0
    )
    normed = rms_scale(all_rows, norm_gain).astype(jnp.bfloat16)
    queries = jnp.dot(normed, query_weight, preferred_element_type=jnp.float32).astype(jnp.bfloat16)
    key_rows = jnp.dot(normed, key_weight, preferred_element_type=jnp.float32).astype(jnp.bfloat16)
    value_rows = jnp.dot(normed, value_weight, preferred_element_type=jnp.float32).astype(
        jnp.bfloat16
    )
    log_gates = jax.nn.log_sigmoid(
        jnp.dot(normed, gate_weight, preferred_element_type=jnp.float32) + gate_bias
    )
    piece_queries = queries[:piece_rows]
    piece_keys = key_rows[:piece_rows].reshape(piece_rows, kv_local, head_dim)
    piece_values = value_rows[:piece_rows].reshape(piece_rows, kv_local, head_dim)
    local_run = jnp.cumsum(log_gates[:piece_rows], axis=0)
    gathered_run = lax.all_gather(local_run, "kv", axis=0, tiled=True)
    shard_run = gathered_run.reshape(kv_count, piece_rows, heads_local)
    totals = shard_run[:, -1]
    before = jnp.cumsum(totals, axis=0) - totals
    piece_run = (shard_run + before[:, None, :]).reshape(kv_count * piece_rows, heads_local)
    own_run = lax.dynamic_slice_in_dim(piece_run, position * piece_rows, piece_rows, 0)
    key_place = position * piece_rows + jnp.arange(piece_rows)
    gate_groups = jnp.moveaxis(past_gate.reshape(kv_local, group_size, -1), 1, 0)
    own_groups = jnp.moveaxis(own_run.reshape(piece_rows, kv_local, group_size), 2, 0)
    shard_queries = lax.all_gather(piece_queries, "kv", axis=0, tiled=True)
    row_count = shard_queries.shape[0]
    query_groups = jnp.moveaxis(
        shard_queries.reshape(row_count, kv_local, group_size, head_dim), 2, 0
    )
    run_groups = jnp.moveaxis(piece_run.reshape(row_count, kv_local, group_size), 2, 0)
    row_place = jnp.arange(row_count)
    causal = key_place[None, :] <= row_place[:, None]

    def one_group(inputs):
        query_one, run_one, gate_one, key_run_one = inputs
        row_bias = run_one.T[:, :, None]
        past_scores = (
            jnp.einsum("nkd,pkd->knp", query_one, past_keys, preferred_element_type=jnp.float32)
            * score_scale
        )
        past_scores = past_scores + gate_one[:, None, :] + row_bias
        new_scores = (
            jnp.einsum("nkd,jkd->knj", query_one, piece_keys, preferred_element_type=jnp.float32)
            * score_scale
        )
        new_scores = new_scores + row_bias - key_run_one.T[:, None, :]
        new_scores = jnp.where(causal[None], new_scores, -jnp.inf)
        row_top = jnp.maximum(jnp.max(past_scores, axis=-1), jnp.max(new_scores, axis=-1))
        past_exp = jnp.exp(past_scores - row_top[..., None])
        new_exp = jnp.exp(new_scores - row_top[..., None])
        row_total = jnp.sum(past_exp, axis=-1) + jnp.sum(new_exp, axis=-1)
        summed = jnp.einsum(
            "knp,pkd->nkd",
            past_exp.astype(jnp.bfloat16),
            past_values,
            preferred_element_type=jnp.float32,
        )
        summed = summed + jnp.einsum(
            "knj,jkd->nkd",
            new_exp.astype(jnp.bfloat16),
            piece_values,
            preferred_element_type=jnp.float32,
        )
        return (summed, row_top.T, row_total.T)

    group_out, group_top, group_total = lax.map(
        one_group, (query_groups, run_groups, gate_groups, own_groups)
    )
    group_out = jnp.moveaxis(group_out, 0, 2).reshape(row_count, heads_local, head_dim)
    group_top = jnp.moveaxis(group_top, 0, 2).reshape(row_count, heads_local)
    group_total = jnp.moveaxis(group_total, 0, 2).reshape(row_count, heads_local)
    arrived = (
        lax.all_to_all(
            group_out.reshape(kv_count, piece_rows, heads_local, head_dim),
            "kv",
            split_axis=0,
            concat_axis=0,
            tiled=True,
        ),
        lax.all_to_all(
            group_top.reshape(kv_count, piece_rows, heads_local),
            "kv",
            split_axis=0,
            concat_axis=0,
            tiled=True,
        ),
        lax.all_to_all(
            group_total.reshape(kv_count, piece_rows, heads_local),
            "kv",
            split_axis=0,
            concat_axis=0,
            tiled=True,
        ),
    )
    global_top = jnp.max(arrived[1], axis=0)
    weights = jnp.exp(arrived[1] - global_top)
    row_total = jnp.sum(arrived[2] * weights, axis=0)
    piece_result = jnp.sum(arrived[0] * weights[..., None], axis=0) / row_total[..., None]
    piece_attention = piece_result.reshape(piece_rows, heads_local * head_dim).astype(jnp.bfloat16)
    dec_queries = queries[piece_rows:].reshape(seq_count, new_count, kv_local, group_size, head_dim)
    dec_new_keys = key_rows[piece_rows:].reshape(seq_count, new_count, kv_local, head_dim)
    dec_new_values = value_rows[piece_rows:].reshape(seq_count, new_count, kv_local, head_dim)
    dec_run = jnp.cumsum(log_gates[piece_rows:].reshape(seq_count, new_count, heads_local), axis=1)
    past_len = dec_keys.shape[1]
    slot_index = jnp.arange(past_len)
    last_gate = jnp.sum(
        jnp.where(slot_index[None, None, :] == (dec_lengths - 1)[:, None, None], dec_gate, 0.0),
        axis=2,
    )
    query_bias = jnp.moveaxis(dec_run.reshape(seq_count, new_count, kv_local, group_size), 1, 3)
    past_bias = last_gate.reshape(seq_count, kv_local, group_size)[..., None, None]
    dec_gate_groups = dec_gate.reshape(seq_count, kv_local, group_size, past_len)
    new_scores = (
        jnp.einsum(
            "stkgd,sukd->skgtu", dec_queries, dec_new_keys, preferred_element_type=jnp.float32
        )
        * score_scale
    )
    new_scores = new_scores + query_bias[..., None] - query_bias[..., None, :]
    new_causal = jnp.arange(new_count)[None, :] <= jnp.arange(new_count)[:, None]
    new_scores = jnp.where(new_causal, new_scores, -jnp.inf)
    new_top = jnp.max(new_scores, axis=-1)
    new_exp = jnp.exp(new_scores - new_top[..., None])
    start_dec = (
        jnp.einsum(
            "skgtu,sukd->skgtd",
            new_exp.astype(jnp.bfloat16),
            dec_new_values,
            preferred_element_type=jnp.float32,
        ),
        new_top,
        jnp.sum(new_exp, axis=-1),
    )
    block_scores = (
        jnp.einsum("stkgd,spkd->skgtp", dec_queries, dec_keys, preferred_element_type=jnp.float32)
        * score_scale
    )
    block_scores = (
        block_scores + query_bias[..., None] + past_bias - dec_gate_groups[:, :, :, None, :]
    )
    live_mask = jnp.arange(past_len)[None, :] < dec_lengths[:, None]
    block_scores = jnp.where(live_mask[:, None, None, None, :], block_scores, -jnp.inf)
    row_top = jnp.maximum(start_dec[1], jnp.max(block_scores, axis=-1))
    block_exp = jnp.exp(block_scores - row_top[..., None])
    rescale = jnp.exp(start_dec[1] - row_top)
    summed = start_dec[0] * rescale[..., None] + jnp.einsum(
        "skgtp,spkd->skgtd",
        block_exp.astype(jnp.bfloat16),
        dec_values,
        preferred_element_type=jnp.float32,
    )
    dec_attention = summed / (start_dec[2] * rescale + jnp.sum(block_exp, axis=-1))[..., None]
    dec_attention = (
        jnp.transpose(dec_attention, (0, 3, 1, 2, 4))
        .reshape(seq_count * new_count, heads_local * head_dim)
        .astype(jnp.bfloat16)
    )
    attention = jnp.concatenate([piece_attention, dec_attention], axis=0)
    partial_rows = jnp.dot(attention, out_weight, preferred_element_type=jnp.float32)
    mixed = lax.psum(partial_rows.astype(jnp.bfloat16), "tp").astype(jnp.float32)
    final_rows = rms_scale(mixed, out_gain).astype(jnp.bfloat16)
    return (
        final_rows[:piece_rows],
        final_rows[piece_rows:].reshape(seq_count, new_count, model_width),
    )


def solution(mesh):
    return jax.shard_map(
        body,
        mesh=mesh,
        in_specs=(
            P(("dp", "kv"), None),
            P(("dp", "kv"), None, None),
            P(),
            P(None, "tp"),
            P(None, "tp"),
            P(None, "tp"),
            P(None, "tp"),
            P("tp"),
            P("tp", None),
            P(),
            P(("dp", "kv"), "tp", None),
            P(("dp", "kv"), "tp", None),
            P("tp", ("dp", "kv")),
            P(("dp", "kv"), None, "tp", None),
            P(("dp", "kv"), None, "tp", None),
            P(("dp", "kv"), "tp", None),
            P(("dp", "kv")),
        ),
        out_specs=(P(("dp", "kv"), None), P(("dp", "kv"), None, None)),
        check_vma=False,
    )
```

profile of v0, /device:TPU:0, one launch (start us, length us, event | category | flops | bytes accessed | tf_op | source)
XLA Modules:
  0.0 105.0 jit_solution(5508176570152350641)
XLA Ops:
  7.2 1.1 %reshape.318 = bf16[48,2048]{1,0:T(8,128)(2,1)S(1)} reshape(bf16[12,4,2048]{2,1,0:T(4,128)(2,1)} %param.20) | data formatting | bytes 393216 | tf_op jit(solution)/shard_map/reshape | solution.py:47
  8.4 1.0 fusion.69
  9.4 1.1 %fusion.87 = f32[64,4]{0,1:T(4,128)S(1)} fusion(bf16[2048,4]{0,1:T(4,128)(2,1)} %param.25, f32[4]{0:T(128)} %param.26, f32[2048]{0:T(1024)} %param.21, f32[64]{0:T(128)S(1)} %add_rsqrt_fusion.1, bf16[48,2048]{1,0:T(8,128)(2,1)S(1)} %reshape.318, bf16[16,2048]{1,0:T(8,128)(2,1)} %param.19), kind=kOutput, calls=%fused_computation.106 | convolution fusion | flops 1968384 | bytes 288016 | tf_op jit(solution)/shard_map/dot_general | solution.py:56
  10.7 13.6 %all-gather = f32[4,16,4]{1,2,0:T(4,128)S(1)} all-gather(f32[1,16,4]{1,2,0:T(4,128)S(1)} %bitcast.224), channel_id=1, replica_groups=mesh['dp'=4,'kv'=4,'tp'=2] {'kv'}, dimensions={0}, use_global_device_ids=true | all-gather | bytes 1280 | tf_op jit(solution)/shard_map/all_gather | solution.py:62
  24.8 0.9 transpose_reshape.3
  25.6 1.4 %convolution_convert_fusion.3 = bf16[64,128]{1,0:T(8,128)(2,1)S(1)} fusion(bf16[2048,128]{1,0:T(8,128)(2,1)} %param.23, f32[2048]{0:T(1024)} %param.21, f32[64]{0:T(128)S(1)} %add_rsqrt_fusion.1, bf16[48,2048]{1,0:T(8,128)(2,1)S(1)} %reshape.318, bf16[16,2048]{1,0:T(8,128)(2,1)} %param.19), kind=kOutput, calls=%fused_computation.61 | convolution fusion | flops 34480128 | bytes 811264 | tf_op jit(solution)/shard_map/dot_general | solution.py:51
  27.1 0.3 convolution_convert_fusion.2
  27.4 0.5 convolution_convert_fusion.1
  27.9 13.1 %all_gather.6 = bf16[64,512]{1,0:T(8,128)(2,1)S(1)} all-gather(bf16[16,512]{1,0:T(8,128)(2,1)S(1)} %slice.44), channel_id=1, replica_groups=mesh['dp'=4,'kv'=4,'tp'=2] {'kv'}, dimensions={0}, use_global_device_ids=true | all-gather | bytes 81920 | tf_op jit(solution)/shard_map/all_gather | solution.py:71
  41.2 4.4 %while.15 = (s32[]{:T(128)}, f32[4,64,1,128]{3,1,2,0:T(8,128)S(1)}, f32[4,64,1]{1,2,0:T(1,128)S(1)}, f32[4,64,1]{1,2,0:T(1,128)S(1)}, bf16[4,64,1,128]{3,1,2,0:T...) while((s32[]{:T(128)}, f32[4,64,1,128]{3,1,2,0:T(8,128)S(1)}, ...), condition=%wide.region_8.9_spmd.clone, body=%wide.region_3.8_spmd.clone.sunk | while | flops 9062274 | bytes 495149 | solution.py:112
  41.4 0.3 fusion.126
  41.7 0.2 fusion.131
  41.9 0.2 fusion.129
  42.1 0.2 fusion.130
  42.5 0.3 fusion.126
  42.8 0.2 fusion.131
  43.0 0.2 fusion.129
  43.2 0.2 fusion.130
  43.6 0.3 fusion.126
  43.9 0.2 fusion.131
  44.1 0.2 fusion.129
  44.3 0.2 fusion.130
  44.7 0.3 fusion.126
  45.0 0.2 fusion.131
  45.2 0.2 fusion.129
  45.4 0.2 fusion.130
  45.7 0.6 copy.73
  46.3 3.4 %all-to-all-start.1 = ((f32[4,16,4]{1,2,0:T(4,128)}), f32[4,16,4]{1,2,0:T(4,128)S(1)}, u32[]{:S(2)}, u32[]{:S(2)}) async-start(f32[4,16,4]{1,2,0:T(4,128)} %copy.73), calls=%async_computation.1 | async-start | bytes 16384 | tf_op jit(solution)/shard_map/all_to_all | solution.py:126
  50.1 0.6 reduce_window_sum.38
  50.7 0.2 copy.78
  50.9 0.6 fusion.95
  51.6 0.4 copy.80
  52.1 2.0 %fusion.96 = (f32[12,4,4]{1,2,0:T(4,128)S(1)}, f32[12,1,4,4,512]{4,2,3,0,1:T(4,128)S(1)}) fusion(f32[12,4,512]{2,1,0:T(4,128)S(1)} %copy-done.5, f32[12,4]{1,0:T(8,128)S(1)} %select_reduce_fusion, f32[12,4,4]{1,2,0:T(4,128)S(1)} %copy.78, bf16[12,4,4,128]{3,2,1,0:T(4,128)(2,1)S(1)} %reshape.325, bf16[12,512,1,128]{3,1,2,0:T(8,128)(2,1)} %param.32, ...), kind=kOutput, calls=%fused_computation.119 | convolution fusion | flops 25755456 | bytes 2121408 | tf_op jit(solution)/shard_map/stkgd,spkd->skgtp/dot_general | solution.py:181
  54.2 0.3 fusion.77
  54.5 0.2 copy.82
  54.9 0.6 copy.75
  55.7 5.1 %all-to-all-start.2 = ((f32[4,16,4]{1,2,0:T(4,128)}), f32[4,16,4]{1,2,0:T(4,128)S(1)}, u32[]{:S(2)}, u32[]{:S(2)}) async-start(f32[4,16,4]{1,2,0:T(4,128)} %copy.75), calls=%async_computation.2 | async-start | bytes 16384 | tf_op jit(solution)/shard_map/all_to_all | solution.py:133
  60.8 1.8 %fusion.65 = bf16[12,4,1,4,128]{4,1,3,0,2:T(4,128)(2,1)S(1)} fusion(f32[12,4,4,128]{3,2,1,0:T(4,128)S(1)} %convolution_multiply_fusion.2, bf16[12,512,1,128]{3,1,2,0:T(8,128)(2,1)} %param.33, bf16[12,4,4,512]{3,1,2,0:T(4,128)(2,1)S(1)} %get-tuple-element.191, f32[12,4,4]{2,1,0:T(4,128)S(1)} %copy.84), kind=kOutput, calls=%fused_computation.59 | convolution fusion | flops 25239552 | bytes 1917696 | tf_op jit(solution)/shard_map/skgtp,spkd->skgtd/dot_general | solution.py:192
  62.6 0.7 copy.72
  63.3 3.2 %all-to-all-done.2 = f32[4,16,4]{1,2,0:T(4,128)S(1)} async-done(((f32[4,16,4]{1,2,0:T(4,128)}), f32[4,16,4]{1,2,0:T(4,128)S(1)}, u32[]{:S(2)}, u32[]{:S(2)}) %all-to-all-start.2) | async-done | bytes 1056 | tf_op jit(solution)/shard_map/all_to_all | solution.py:133
  66.5 3.3 %all-to-all-start = ((f32[4,16,4,128]{3,1,2,0:T(8,128)}), f32[4,16,4,128]{3,1,2,0:T(8,128)S(1)}, u32[]{:S(2)}, u32[]{:S(2)}) async-start(f32[4,16,4,128]{3,1,2,0:T(8,128)} %copy.72), calls=%async_computation | async-start | bytes 262144 | tf_op jit(solution)/shard_map/all_to_all | solution.py:119
  69.9 5.8 %all-to-all-done = f32[4,16,4,128]{3,1,2,0:T(8,128)S(1)} async-done(((f32[4,16,4,128]{3,1,2,0:T(8,128)}), f32[4,16,4,128]{3,1,2,0:T(8,128)S(1)}, u32[]{:S(2)}, u32[]{:S(2)}) %all-to-all-start) | async-done | bytes 131104 | tf_op jit(solution)/shard_map/all_to_all | solution.py:119
  75.9 1.2 %convolution_convert_fusion = bf16[64,2048]{1,0:T(8,128)(2,1)} fusion(bf16[512,2048]{1,0:T(8,128)(2,1)S(1)} %copy-done, bf16[48,512]{1,0:T(8,128)(2,1)S(1)} %bitcast.214, bf16[16,512]{1,0:T(8,128)(2,1)S(1)} %copy_bitcast_fusion.2), kind=kOutput, calls=%fused_computation.38 | convolution fusion | flops 134479872 | bytes 2424832 | tf_op jit(solution)/shard_map/dot_general | solution.py:205
  77.1 17.4 %all-reduce.2.cloned.1.call-done = bf16[64,2048]{1,0:T(8,128)(2,1)} async-done(((bf16[64,2048]{1,0:T(8,128)(2,1)}), bf16[64,2048]{1,0:T(8,128)(2,1)}) %all-reduce.2.cloned.1.call-update) | async-done | bytes 262160 | tf_op jit(solution)/shard_map/psum | solution.py:206
  94.6 1.1 %fusion.72 = f32[64]{0:T(128)S(1)} fusion(bf16[64,2048]{1,0:T(8,128)(2,1)} %all-reduce.2.cloned.1.call-done), kind=kLoop, calls=%fused_computation.72 | loop fusion | flops 393152 | bytes 262400 | tf_op jit(solution)/shard_map/reduce_sum | solution.py:12
  95.7 1.1 %fusion.74 = bf16[64,2048]{1,0:T(8,128)(2,1)S(1)} fusion(bf16[64,2048]{1,0:T(8,128)(2,1)} %all-reduce.2.cloned.1.call-done, f32[2048]{0:T(1024)S(1)} %copy-done.8, f32[64]{0:T(128)S(1)} %add_rsqrt_fusion), kind=kLoop, calls=%fused_computation.74 | loop fusion | flops 524288 | bytes 532736 | tf_op jit(solution)/shard_map/convert_element_type | solution.py:207
  96.8 0.6 slice.51
  97.4 0.8 reshape.331
  (100 shorter events, 3.1 us)
Async XLA Ops:
  7.2 68.7 %copy-start = (bf16[512,2048]{1,0:T(8,128)(2,1)S(1)}, bf16[512,2048]{1,0:T(8,128)(2,1)}, u32[]{:S(2)}) copy-start(bf16[512,2048]{1,0:T(8,128)(2,1)} %param.27) | copy-start | bytes 6291460
  7.2 19.8 %copy-start.4 = (bf16[16,2048]{1,0:T(8,128)(2,1)S(1)}, bf16[16,2048]{1,0:T(8,128)(2,1)}, u32[]{:S(2)}) copy-start(bf16[16,2048]{1,0:T(8,128)(2,1)} %param.19) | copy-start | bytes 196612
  7.2 19.8 %copy-start.7 = (f32[2048]{0:T(1024)S(1)}, f32[2048]{0:T(1024)}, u32[]{:S(2)}) copy-start(f32[2048]{0:T(1024)} %param.21) | copy-start | bytes 24580
  7.2 19.8 %copy-start.10 = (bf16[2048,128]{1,0:T(8,128)(2,1)S(1)}, bf16[2048,128]{1,0:T(8,128)(2,1)}, u32[]{:S(2)}) copy-start(bf16[2048,128]{1,0:T(8,128)(2,1)} %param.24) | copy-start | bytes 1572868
  24.8 2.6 %copy-start.1 = (bf16[2048,512]{1,0:T(8,128)(2,1)S(1)}, bf16[2048,512]{1,0:T(8,128)(2,1)}, u32[]{:S(2)}) copy-start(bf16[2048,512]{1,0:T(8,128)(2,1)} %param.22) | copy-start | bytes 6291460
  27.0 14.2 %copy-start.2 = (bf16[256,1,128]{2,0,1:T(8,128)(2,1)S(1)}, bf16[256,1,128]{2,0,1:T(8,128)(2,1)}, u32[]{:S(2)}) copy-start(bf16[256,1,128]{2,0,1:T(8,128)(2,1)} %param.29) | copy-start | bytes 196612
  27.0 14.2 %copy-start.3 = (bf16[256,1,128]{2,0,1:T(8,128)(2,1)S(1)}, bf16[256,1,128]{2,0,1:T(8,128)(2,1)}, u32[]{:S(2)}) copy-start(bf16[256,1,128]{2,0,1:T(8,128)(2,1)} %param.30) | copy-start | bytes 196612
  27.4 22.5 %copy-start.6 = (bf16[64,128]{1,0:T(8,128)(2,1)}, bf16[64,128]{1,0:T(8,128)(2,1)S(1)}, u32[]{:S(2)}) copy-start(bf16[64,128]{1,0:T(8,128)(2,1)S(1)} %convolution_convert_fusion.2) | copy-start | bytes 49156
  27.9 21.8 %copy-start.9 = (s32[12]{0:T(128)S(1)}, s32[12]{0:T(128)}, u32[]{:S(2)}) copy-start(s32[12]{0:T(128)} %param.35) | copy-start | bytes 148
  41.2 10.8 %copy-start.5 = (f32[12,4,512]{2,1,0:T(4,128)S(1)}, f32[12,4,512]{2,1,0:T(4,128)}, u32[]{:S(2)}) copy-start(f32[12,4,512]{2,1,0:T(4,128)} %param.34) | copy-start | bytes 294916
  46.3 9.4 %all-to-all-start.1 = ((f32[4,16,4]{1,2,0:T(4,128)}), f32[4,16,4]{1,2,0:T(4,128)S(1)}, u32[]{:S(2)}, u32[]{:S(2)}) async-start(f32[4,16,4]{1,2,0:T(4,128)} %copy.73), calls=%async_computation.1 | async-start | bytes 16384 | tf_op jit(solution)/shard_map/all_to_all | solution.py:126
  50.1 4.6 %slice-start = ((bf16[64,128]{1,0:T(8,128)(2,1)}), bf16[48,128]{1,0:T(8,128)(2,1)S(1)}, s32[]{:S(2)}) async-start(bf16[64,128]{1,0:T(8,128)(2,1)} %copy-done.6), calls=%async_computation.4 | async-start | bytes 24576 | tf_op jit(solution)/shard_map/slice | solution.py:148
  55.7 10.8 %all-to-all-start.2 = ((f32[4,16,4]{1,2,0:T(4,128)}), f32[4,16,4]{1,2,0:T(4,128)S(1)}, u32[]{:S(2)}, u32[]{:S(2)}) async-start(f32[4,16,4]{1,2,0:T(4,128)} %copy.75), calls=%async_computation.2 | async-start | bytes 16384 | tf_op jit(solution)/shard_map/all_to_all | solution.py:133
  62.6 33.1 %copy-start.8 = (f32[2048]{0:T(1024)S(1)}, f32[2048]{0:T(1024)}, u32[]{:S(2)}) copy-start(f32[2048]{0:T(1024)} %param.28) | copy-start | bytes 24580
  66.5 9.2 %all-to-all-start = ((f32[4,16,4,128]{3,1,2,0:T(8,128)}), f32[4,16,4,128]{3,1,2,0:T(8,128)S(1)}, u32[]{:S(2)}, u32[]{:S(2)}) async-start(f32[4,16,4,128]{3,1,2,0:T(8,128)} %copy.72), calls=%async_computation | async-start | bytes 262144 | tf_op jit(solution)/shard_map/all_to_all | solution.py:119
  69.8 24.7 %all-reduce.2.cloned.1.call-start = ((), (), s32[]{:S(2)}) async-start(), calls=%async_computation.3 | async-start | bytes 524288 | tf_op jit(solution)/shard_map/psum | solution.py:206
Sparse Core Ops, SparseCore 0:
  77.2 17.2 all-reduce.1
where the time goes:
time: 106 us; the launch traced here: 105 us
  blocking collectives  26.8 us (25%)
  waiting for transfers between devices  26.5 us (25%)
  between operations  14.4 us (14%)
  matrix products  12.2 us (12%)
  starting transfers between devices  11.9 us (11%)
  local copies, waits for them, and re-layouts  7.15 us (7%)
  other arithmetic  6.01 us (6%)
    psum x1, waiting for transfers between devices, body(): lax.psum(partial_rows.astype(jnp.bfloat16), 'tp').astype(jnp.float32)  17.4 us
    all_gather x1, blocking collectives, body(): gathered_run = lax.all_gather(local_run, 'kv', axis=0, tiled=True)  13.6 us
    all_gather x1, blocking collectives, body(): shard_queries = lax.all_gather(piece_queries, 'kv', axis=0, tiled=True)  13.1 us
    all_to_all x1, waiting for transfers between devices, body(): lax.all_to_all(group_out.reshape(kv_count, piece_rows, heads_local, head_...  5.81 us
    all_to_all x1, starting transfers between devices, body(): lax.all_to_all(group_total.reshape(kv_count, piece_rows, heads_local), 'k...  5.09 us
    all_to_all x1, starting transfers between devices, body(): lax.all_to_all(group_top.reshape(kv_count, piece_rows, heads_local), 'kv'...  3.44 us
    all_to_all x1, starting transfers between devices, body(): lax.all_to_all(group_out.reshape(kv_count, piece_rows, heads_local, head_...  3.33 us
    all_to_all x1, waiting for transfers between devices, body(): lax.all_to_all(group_total.reshape(kv_count, piece_rows, heads_local), 'k...  3.19 us
  transfers between devices with their start and end apart: 4, of which 3 were waited for; matrix products, arithmetic and copies ran while one was open for 8% of the time, Pallas kernels for 0%

commit v1 on v0

--- a/solution.py
+++ b/solution.py
@@ -203,7 +203,9 @@
     )
     attention = jnp.concatenate([piece_attention, dec_attention], axis=0)
     partial_rows = jnp.dot(attention, out_weight, preferred_element_type=jnp.float32)
-    mixed = lax.psum(partial_rows.astype(jnp.bfloat16), "tp").astype(jnp.float32)
+    mixed = jnp.sum(lax.all_gather(partial_rows.astype(jnp.bfloat16), "tp"), axis=0).astype(
+        jnp.float32
+    )
     final_rows = rms_scale(mixed, out_gain).astype(jnp.bfloat16)
     return (
         final_rows[:piece_rows],

time: 106 us -> 74.5 us (0.70)
  waiting for transfers between devices: 26.5 us -> 9.07 us
  between operations: 14.4 us -> 0.99 us
  blocking collectives: 26.8 us -> 28.9 us
  other arithmetic: 6.01 us -> 4.24 us
    psum x1 -> x0, waiting for transfers between devices: 17.4 us -> none  [body(): lax.psum(partial_rows.astype(jnp.bfloat16), 'tp').astype(jnp.float32)]
    all_gather x0 -> x1, blocking collectives: none -> 2.18 us  [body(): lax.all_gather(partial_rows.astype(jnp.bfloat16), 'tp')]
  transfers between devices with their start and end apart: 4 -> 3, of which waited for: 3 -> 2; matrix products, arithmetic and copies ran while one was open for 8% -> 11% of each run, Pallas kernels for 0% -> 0%
where the time goes in v1:
time: 74.5 us; the launch traced here: 73.9 us
  blocking collectives  28.9 us (39%)
  starting transfers between devices  11.9 us (16%)
  matrix products  11.5 us (15%)
  waiting for transfers between devices  9.07 us (12%)
  local copies, waits for them, and re-layouts  7.16 us (10%)
  other arithmetic  4.24 us (6%)
  between operations  0.99 us (1%)
    all_gather x1, blocking collectives, body(): gathered_run = lax.all_gather(local_run, 'kv', axis=0, tiled=True)  13.6 us
    all_gather x1, blocking collectives, body(): shard_queries = lax.all_gather(piece_queries, 'kv', axis=0, tiled=True)  13.1 us
    all_to_all x1, waiting for transfers between devices, body(): lax.all_to_all(group_out.reshape(kv_count, piece_rows, heads_local, head_...  5.86 us
    all_to_all x1, starting transfers between devices, body(): lax.all_to_all(group_total.reshape(kv_count, piece_rows, heads_local), 'k...  5.09 us
    all_to_all x1, starting transfers between devices, body(): lax.all_to_all(group_top.reshape(kv_count, piece_rows, heads_local), 'kv'...  3.44 us
    all_to_all x1, starting transfers between devices, body(): lax.all_to_all(group_out.reshape(kv_count, piece_rows, heads_local, head_...  3.33 us
    all_to_all x1, waiting for transfers between devices, body(): lax.all_to_all(group_total.reshape(kv_count, piece_rows, heads_local), 'k...  3.2 us
    all_gather x1, blocking collectives, body(): lax.all_gather(partial_rows.astype(jnp.bfloat16), 'tp')  2.18 us
  transfers between devices with their start and end apart: 3, of which 2 were waited for; matrix products, arithmetic and copies ran while one was open for 11% of the time, Pallas kernels for 0%

profile of v1, /device:TPU:0, one launch (start us, length us, event | category | flops | bytes accessed | tf_op | source)
XLA Modules:
  0.0 73.9 jit_solution(9545910285803503520)
XLA Ops:
  0.7 1.1 %reshape.318 = bf16[48,2048]{1,0:T(8,128)(2,1)S(1)} reshape(bf16[12,4,2048]{2,1,0:T(4,128)(2,1)} %param.20) | data formatting | bytes 393216 | tf_op jit(solution)/shard_map/reshape | solution.py:47
  1.8 1.0 %fusion.69 = f32[64]{0:T(128)S(1)} fusion(bf16[48,2048]{1,0:T(8,128)(2,1)S(1)} %reshape.318, bf16[16,2048]{1,0:T(8,128)(2,1)} %param.19), kind=kLoop, calls=%fused_computation.69 | loop fusion | flops 786368 | bytes 262400 | tf_op jit(solution)/shard_map/reduce_sum | solution.py:12
  2.9 1.1 %fusion.87 = f32[64,4]{0,1:T(4,128)S(1)} fusion(bf16[2048,4]{0,1:T(4,128)(2,1)} %param.25, f32[4]{0:T(128)} %param.26, f32[2048]{0:T(1024)} %param.21, f32[64]{0:T(128)S(1)} %add_rsqrt_fusion.1, bf16[48,2048]{1,0:T(8,128)(2,1)S(1)} %reshape.318, bf16[16,2048]{1,0:T(8,128)(2,1)} %param.19), kind=kOutput, calls=%fused_computation.106 | convolution fusion | flops 1968384 | bytes 288016 | tf_op jit(solution)/shard_map/dot_general | solution.py:56
  4.2 13.6 %all-gather.1 = f32[4,16,4]{1,2,0:T(4,128)S(1)} all-gather(f32[1,16,4]{1,2,0:T(4,128)S(1)} %bitcast.226), channel_id=1, replica_groups=mesh['dp'=4,'kv'=4,'tp'=2] {'kv'}, dimensions={0}, use_global_device_ids=true | all-gather | bytes 1280 | tf_op jit(solution)/shard_map/all_gather | solution.py:62
  17.8 0.2 fusion.97
  18.2 0.9 %transpose_reshape.3 = f32[4,1,256]{2,1,0:T(1,128)S(1)} reshape(f32[4,256]{1,0:T(4,128)} %param.31) | data formatting | bytes 8192 | tf_op jit(solution)/shard_map/transpose;reshape | solution.py:69
  19.1 1.4 %convolution_convert_fusion.3 = bf16[64,128]{1,0:T(8,128)(2,1)S(1)} fusion(bf16[2048,128]{1,0:T(8,128)(2,1)} %param.23, f32[2048]{0:T(1024)} %param.21, f32[64]{0:T(128)S(1)} %add_rsqrt_fusion.1, bf16[48,2048]{1,0:T(8,128)(2,1)S(1)} %reshape.318, bf16[16,2048]{1,0:T(8,128)(2,1)} %param.19), kind=kOutput, calls=%fused_computation.61 | convolution fusion | flops 34480128 | bytes 811264 | tf_op jit(solution)/shard_map/dot_general | solution.py:51
  20.5 0.3 convolution_convert_fusion.2
  20.8 0.5 convolution_convert_fusion.1
  21.4 13.1 %all_gather.12 = bf16[64,512]{1,0:T(8,128)(2,1)S(1)} all-gather(bf16[16,512]{1,0:T(8,128)(2,1)S(1)} %slice.44), channel_id=1, replica_groups=mesh['dp'=4,'kv'=4,'tp'=2] {'kv'}, dimensions={0}, use_global_device_ids=true | all-gather | bytes 81920 | tf_op jit(solution)/shard_map/all_gather | solution.py:71
  34.6 4.4 %while.15 = (s32[]{:T(128)}, f32[4,64,1,128]{3,1,2,0:T(8,128)S(1)}, f32[4,64,1]{1,2,0:T(1,128)S(1)}, f32[4,64,1]{1,2,0:T(1,128)S(1)}, bf16[4,64,1,128]{3,1,2,0:T...) while((s32[]{:T(128)}, f32[4,64,1,128]{3,1,2,0:T(8,128)S(1)}, ...), condition=%wide.region_8.9_spmd.clone, body=%wide.region_3.8_spmd.clone.sunk | while | flops 9062274 | bytes 495149 | solution.py:112
  34.8 0.3 fusion.126
  35.1 0.2 fusion.131
  35.3 0.2 fusion.129
  35.6 0.2 fusion.130
  35.9 0.3 fusion.126
  36.2 0.2 fusion.131
  36.4 0.2 fusion.129
  36.7 0.2 fusion.130
  37.0 0.3 fusion.126
  37.3 0.2 fusion.131
  37.5 0.2 fusion.129
  37.7 0.2 fusion.130
  38.1 0.3 fusion.126
  38.4 0.2 fusion.131
  38.6 0.2 fusion.129
  38.8 0.2 fusion.130
  39.1 0.6 copy.73
  39.7 3.4 %all-to-all-start.1 = ((f32[4,16,4]{1,2,0:T(4,128)}), f32[4,16,4]{1,2,0:T(4,128)S(1)}, u32[]{:S(2)}, u32[]{:S(2)}) async-start(f32[4,16,4]{1,2,0:T(4,128)} %copy.73), calls=%async_computation.1 | async-start | bytes 16384 | tf_op jit(solution)/shard_map/all_to_all | solution.py:126
  43.6 0.6 reduce_window_sum.38
  44.2 0.2 copy.78
  44.4 0.6 fusion.95
  45.1 0.4 copy.80
  45.6 2.0 %fusion.96 = (f32[12,4,4]{1,2,0:T(4,128)S(1)}, f32[12,1,4,4,512]{4,2,3,0,1:T(4,128)S(1)}) fusion(f32[12,4,512]{2,1,0:T(4,128)S(1)} %copy-done.5, f32[12,4]{1,0:T(8,128)S(1)} %select_reduce_fusion, f32[12,4,4]{1,2,0:T(4,128)S(1)} %copy.78, bf16[12,4,4,128]{3,2,1,0:T(4,128)(2,1)S(1)} %reshape.325, bf16[12,512,1,128]{3,1,2,0:T(8,128)(2,1)} %param.32, ...), kind=kOutput, calls=%fused_computation.119 | convolution fusion | flops 25755456 | bytes 2121408 | tf_op jit(solution)/shard_map/stkgd,spkd->skgtp/dot_general | solution.py:181
  47.7 0.3 fusion.77
  48.0 0.2 copy.82
  48.4 0.6 copy.75
  49.0 0.2 copy.84
  49.2 5.1 %all-to-all-start.2 = ((f32[4,16,4]{1,2,0:T(4,128)}), f32[4,16,4]{1,2,0:T(4,128)S(1)}, u32[]{:S(2)}, u32[]{:S(2)}) async-start(f32[4,16,4]{1,2,0:T(4,128)} %copy.75), calls=%async_computation.2 | async-start | bytes 16384 | tf_op jit(solution)/shard_map/all_to_all | solution.py:133
  54.3 1.8 %fusion.65 = bf16[12,4,1,4,128]{4,1,3,0,2:T(4,128)(2,1)S(1)} fusion(f32[12,4,4,128]{3,2,1,0:T(4,128)S(1)} %convolution_multiply_fusion.2, bf16[12,512,1,128]{3,1,2,0:T(8,128)(2,1)} %param.33, bf16[12,4,4,512]{3,1,2,0:T(4,128)(2,1)S(1)} %get-tuple-element.191, f32[12,4,4]{2,1,0:T(4,128)S(1)} %copy.84), kind=kOutput, calls=%fused_computation.59 | convolution fusion | flops 25239552 | bytes 1917696 | tf_op jit(solution)/shard_map/skgtp,spkd->skgtd/dot_general | solution.py:192
  56.0 0.7 copy.72
  56.8 3.2 %all-to-all-done.2 = f32[4,16,4]{1,2,0:T(4,128)S(1)} async-done(((f32[4,16,4]{1,2,0:T(4,128)}), f32[4,16,4]{1,2,0:T(4,128)S(1)}, u32[]{:S(2)}, u32[]{:S(2)}) %all-to-all-start.2) | async-done | bytes 1056 | tf_op jit(solution)/shard_map/all_to_all | solution.py:133
  60.0 3.3 %all-to-all-start = ((f32[4,16,4,128]{3,1,2,0:T(8,128)}), f32[4,16,4,128]{3,1,2,0:T(8,128)S(1)}, u32[]{:S(2)}, u32[]{:S(2)}) async-start(f32[4,16,4,128]{3,1,2,0:T(8,128)} %copy.72), calls=%async_computation | async-start | bytes 262144 | tf_op jit(solution)/shard_map/all_to_all | solution.py:119
  63.3 5.9 %all-to-all-done = f32[4,16,4,128]{3,1,2,0:T(8,128)S(1)} async-done(((f32[4,16,4,128]{3,1,2,0:T(8,128)}), f32[4,16,4,128]{3,1,2,0:T(8,128)S(1)}, u32[]{:S(2)}, u32[]{:S(2)}) %all-to-all-start) | async-done | bytes 131104 | tf_op jit(solution)/shard_map/all_to_all | solution.py:119
  69.4 0.5 convolution_convert_fusion
  69.9 2.2 %all-gather = bf16[128,2048]{1,0:T(8,128)(2,1)S(1)} all-gather(bf16[64,2048]{1,0:T(8,128)(2,1)S(1)} %convolution_convert_fusion), channel_id=2, replica_groups=mesh['dp'=4,'kv'=4,'tp'=2] {'tp'}, dimensions={0}, use_global_device_ids=true | all-gather | bytes 786432 | tf_op jit(solution)/shard_map/all_gather | solution.py:206
  72.5 0.6 slice.51
  73.1 0.8 %reshape.331 = bf16[12,4,2048]{2,1,0:T(4,128)(2,1)} reshape(bf16[48,2048]{1,0:T(8,128)(2,1)S(1)} %slice.52) | data formatting | bytes 393216 | tf_op jit(solution)/shard_map/reshape | solution.py:212
  (99 shorter events, 3.1 us)
Async XLA Ops:
  0.6 68.7 %copy-start = (bf16[512,2048]{1,0:T(8,128)(2,1)S(1)}, bf16[512,2048]{1,0:T(8,128)(2,1)}, u32[]{:S(2)}) copy-start(bf16[512,2048]{1,0:T(8,128)(2,1)} %param.27) | copy-start | bytes 6291460
  0.6 19.8 %copy-start.4 = (bf16[16,2048]{1,0:T(8,128)(2,1)S(1)}, bf16[16,2048]{1,0:T(8,128)(2,1)}, u32[]{:S(2)}) copy-start(bf16[16,2048]{1,0:T(8,128)(2,1)} %param.19) | copy-start | bytes 196612
  0.7 19.8 %copy-start.7 = (f32[2048]{0:T(1024)S(1)}, f32[2048]{0:T(1024)}, u32[]{:S(2)}) copy-start(f32[2048]{0:T(1024)} %param.21) | copy-start | bytes 24580
  0.7 19.8 %copy-start.10 = (bf16[2048,128]{1,0:T(8,128)(2,1)S(1)}, bf16[2048,128]{1,0:T(8,128)(2,1)}, u32[]{:S(2)}) copy-start(bf16[2048,128]{1,0:T(8,128)(2,1)} %param.24) | copy-start | bytes 1572868
  18.2 2.6 %copy-start.1 = (bf16[2048,512]{1,0:T(8,128)(2,1)S(1)}, bf16[2048,512]{1,0:T(8,128)(2,1)}, u32[]{:S(2)}) copy-start(bf16[2048,512]{1,0:T(8,128)(2,1)} %param.22) | copy-start | bytes 6291460
  20.5 14.2 %copy-start.2 = (bf16[256,1,128]{2,0,1:T(8,128)(2,1)S(1)}, bf16[256,1,128]{2,0,1:T(8,128)(2,1)}, u32[]{:S(2)}) copy-start(bf16[256,1,128]{2,0,1:T(8,128)(2,1)} %param.29) | copy-start | bytes 196612
  20.5 14.2 %copy-start.3 = (bf16[256,1,128]{2,0,1:T(8,128)(2,1)S(1)}, bf16[256,1,128]{2,0,1:T(8,128)(2,1)}, u32[]{:S(2)}) copy-start(bf16[256,1,128]{2,0,1:T(8,128)(2,1)} %param.30) | copy-start | bytes 196612
  20.8 22.5 %copy-start.6 = (bf16[64,128]{1,0:T(8,128)(2,1)}, bf16[64,128]{1,0:T(8,128)(2,1)S(1)}, u32[]{:S(2)}) copy-start(bf16[64,128]{1,0:T(8,128)(2,1)S(1)} %convolution_convert_fusion.2) | copy-start | bytes 49156
  21.4 21.8 %copy-start.9 = (s32[12]{0:T(128)S(1)}, s32[12]{0:T(128)}, u32[]{:S(2)}) copy-start(s32[12]{0:T(128)} %param.35) | copy-start | bytes 148
  34.6 10.8 %copy-start.5 = (f32[12,4,512]{2,1,0:T(4,128)S(1)}, f32[12,4,512]{2,1,0:T(4,128)}, u32[]{:S(2)}) copy-start(f32[12,4,512]{2,1,0:T(4,128)} %param.34) | copy-start | bytes 294916
  39.7 9.4 %all-to-all-start.1 = ((f32[4,16,4]{1,2,0:T(4,128)}), f32[4,16,4]{1,2,0:T(4,128)S(1)}, u32[]{:S(2)}, u32[]{:S(2)}) async-start(f32[4,16,4]{1,2,0:T(4,128)} %copy.73), calls=%async_computation.1 | async-start | bytes 16384 | tf_op jit(solution)/shard_map/all_to_all | solution.py:126
  43.5 4.6 %slice-start = ((bf16[64,128]{1,0:T(8,128)(2,1)}), bf16[48,128]{1,0:T(8,128)(2,1)S(1)}, s32[]{:S(2)}) async-start(bf16[64,128]{1,0:T(8,128)(2,1)} %copy-done.6), calls=%async_computation.3 | async-start | bytes 24576 | tf_op jit(solution)/shard_map/slice | solution.py:148
  49.2 10.8 %all-to-all-start.2 = ((f32[4,16,4]{1,2,0:T(4,128)}), f32[4,16,4]{1,2,0:T(4,128)S(1)}, u32[]{:S(2)}, u32[]{:S(2)}) async-start(f32[4,16,4]{1,2,0:T(4,128)} %copy.75), calls=%async_computation.2 | async-start | bytes 16384 | tf_op jit(solution)/shard_map/all_to_all | solution.py:133
  60.0 9.2 %all-to-all-start = ((f32[4,16,4,128]{3,1,2,0:T(8,128)}), f32[4,16,4,128]{3,1,2,0:T(8,128)S(1)}, u32[]{:S(2)}, u32[]{:S(2)}) async-start(f32[4,16,4,128]{3,1,2,0:T(8,128)} %copy.72), calls=%async_computation | async-start | bytes 262144 | tf_op jit(solution)/shard_map/all_to_all | solution.py:119
  69.4 3.0 %copy-start.8 = (f32[2048]{0:T(1024)S(1)}, f32[2048]{0:T(1024)}, u32[]{:S(2)}) copy-start(f32[2048]{0:T(1024)} %param.28) | copy-start | bytes 24580
